TPU v7x, 32 devices: a whole 2x2x4 slice. The times are simulated.
32 devices in a mesh: sp: 8 (over z, x), tp: 4 (over y, core).
Axes of the slice: x: 2, y: 2, z: 4, core: 2. Of those that a mesh axis runs over, the one named last changes fastest.
Arguments:
- tokens: bfloat16 [1024, 1024], P('sp', 'tp'), may hold values from -6 to 6
- norm_gain: float32 [3, 1024], replicated, may hold values from 0.1 to 1.9
- w_query: bfloat16 [3, 1024, 1024], P(None, 'sp', 'tp'), may hold values from -0.1875 to 0.1875
- w_key: bfloat16 [3, 1024, 1024], P(None, 'sp', 'tp'), may hold values from -0.1875 to 0.1875
- w_value: bfloat16 [3, 1024, 1024], P(None, 'sp', 'tp'), may hold values from -0.1875 to 0.1875
- w_out: bfloat16 [3, 1024, 1024], P(None, 'tp', 'sp'), may hold values from -0.5625 to 0.5625
- offset_bias: float32 [3, 16, 8, 16], P(None, 'tp'), may hold values from -3 to 3
- documents: int32 [1024], P('sp'), may hold values from 0 to 7, never falling along the last dimension, each value on 1 to 256 neighbouring positions
Outputs:
- mixed: bfloat16 [1024, 1024], P('sp', 'tp')
Inputs may be any that keep to these rules, and one draw needn't show every extreme that they name: `documents`: document numbers never fall along the token order, start at 0, and each document has 1 to 256 tokens.
All inputs are finite; a program needn't handle non-finite values.
Results may differ from a plain program's by a relative error of at most 0.02.
Values may be sent and summed in bfloat16 or wider, within the bound.
A program may use at most 64 MiB of HBM per device.

v0:
```python
import jax
import jax.numpy as jnp
from jax import lax
from jax.sharding import PartitionSpec as P

HEAD_DIM = 64
WIN_ROWS = 8
WIN_COLS = 16
LAYERS = 3
GRID_W = 32
EPS = 1e-06


def with_halo(shard, sides, width, wrap):
    for axis, dim in sides:
        count, length = (lax.axis_size(axis), shard.shape[dim])
        up = [(i, (i + 1) % count) for i in range(count if wrap else count - 1)]
        down = [(j, i) for i, j in up]
        last = lax.slice_in_dim(shard, length - width, length, axis=dim)
        leading = lax.slice_in_dim(shard, 0, width, axis=dim)
        before = lax.ppermute(last, axis, up)
        after = lax.ppermute(leading, axis, down)
        shard = jnp.concatenate([before, shard, after], axis=dim)
    return shard


def rms_rows(stream, gain_row):
    values = stream.astype(jnp.float32)
    mean_sq = jnp.mean(values * values, axis=-1, keepdims=True)
    return (values * lax.rsqrt(mean_sq + EPS) * gain_row).astype(jnp.bfloat16)


def head_norm(heads_raw):
    values = heads_raw.astype(jnp.float32)
    mean_sq = jnp.mean(values * values, axis=-1, keepdims=True)
    return (values * lax.rsqrt(mean_sq + EPS)).astype(jnp.bfloat16)


def attend(queries, fringe, seg_own, seg_fringe, bias_layer):
    row_count, grid_width, head_count, head_width = queries.shape
    key_rows = jnp.stack(
        [fringe[row_lag : row_lag + row_count] for row_lag in range(WIN_ROWS)], axis=1
    )
    seg_rows = jnp.stack(
        [seg_fringe[row_lag : row_lag + row_count] for row_lag in range(WIN_ROWS)], axis=1
    )
    key_part = key_rows[..., :head_width]
    value_part = key_rows[..., head_width:]
    scores = jnp.einsum(
        "rchd,rjkhd->rhcjk", queries, key_part, preferred_element_type=jnp.float32
    ) * head_width ** (-0.5)
    column = jnp.arange(grid_width)
    col_offset = column[None, :] - column[:, None] + WIN_COLS // 2
    inside = (col_offset >= 0) & (col_offset < WIN_COLS)
    bias_table = bias_layer[:, :, jnp.clip(col_offset, 0, WIN_COLS - 1)]
    scores = scores + jnp.transpose(bias_table, (0, 2, 1, 3))[None]
    same_doc = seg_rows[:, None, None, :, :] == seg_own[:, None, :, None, None]
    allowed = same_doc & inside[None, None, :, None, :]
    scores = jnp.where(allowed, scores, -1e30)
    flat = scores.reshape(row_count, head_count, grid_width, WIN_ROWS * grid_width)
    attn_probs = jax.nn.softmax(flat, axis=-1).astype(jnp.bfloat16)
    attn_probs = attn_probs.reshape(row_count, head_count, grid_width, WIN_ROWS, grid_width)
    mixed_heads = jnp.einsum(
        "rhcjk,rjkhd->rchd", attn_probs, value_part, preferred_element_type=jnp.float32
    )
    return mixed_heads.astype(jnp.bfloat16)


def body(tokens, norm_gain, w_query, w_key, w_value, w_out, offset_bias, documents):
    token_count = tokens.shape[0]
    row_count = token_count // GRID_W
    reach_rows = WIN_ROWS // 2
    head_count = offset_bias.shape[1]
    seg_own = (documents + 1).reshape(row_count, GRID_W)
    seg_fringe = with_halo(seg_own, (("sp", 0),), reach_rows, False)
    collected = (
        lax.all_gather(w_query, "sp", axis=1, tiled=True),
        lax.all_gather(w_key, "sp", axis=1, tiled=True),
        lax.all_gather(w_value, "sp", axis=1, tiled=True),
        lax.all_gather(w_out, "sp", axis=2, tiled=True),
    )
    stream = tokens
    for layer_index in range(LAYERS):
        gathered = lax.all_gather(stream, "tp", axis=1, tiled=True)
        normed = rms_rows(gathered, norm_gain[layer_index])
        query_raw = jnp.dot(normed, collected[0][layer_index], preferred_element_type=jnp.float32)
        key_raw = jnp.dot(normed, collected[1][layer_index], preferred_element_type=jnp.float32)
        value_raw = jnp.dot(normed, collected[2][layer_index], preferred_element_type=jnp.float32)
        query_heads = head_norm(
            query_raw.astype(jnp.bfloat16).reshape(row_count, GRID_W, head_count, HEAD_DIM)
        )
        key_heads = head_norm(
            key_raw.astype(jnp.bfloat16).reshape(row_count, GRID_W, head_count, HEAD_DIM)
        )
        value_heads = value_raw.astype(jnp.bfloat16).reshape(
            row_count, GRID_W, head_count, HEAD_DIM
        )
        key_value = jnp.concatenate([key_heads, value_heads], axis=-1)
        fringe = with_halo(key_value, (("sp", 0),), reach_rows, False)
        attended = attend(query_heads, fringe, seg_own, seg_fringe, offset_bias[layer_index])
        attended = attended.reshape(token_count, head_count * HEAD_DIM)
        partial_sums = jnp.dot(
            attended, collected[3][layer_index], preferred_element_type=jnp.float32
        )
        stream = (
            lax.psum_scatter(
                partial_sums.astype(jnp.bfloat16), "tp", scatter_dimension=1, tiled=True
            )
            .astype(jnp.float32)
            .astype(jnp.bfloat16)
        )
    return stream


def solution(mesh):
    return jax.shard_map(
        body,
        mesh=mesh,
        in_specs=(
            P("sp", "tp"),
            P(),
            P(None, "sp", "tp"),
            P(None, "sp", "tp"),
            P(None, "sp", "tp"),
            P(None, "tp", "sp"),
            P(None, "tp", None, None),
            P("sp"),
        ),
        out_specs=P("sp", "tp"),
        check_vma=False,
    )
```

profile of v0, /device:TPU:0, one launch (start us, length us, event | category | flops | bytes accessed | tf_op | source)
XLA Modules:
  0.0 309.1 jit_solution(167499018848324964)
XLA Ops:
  9.5 4.9 %collective-permute-start.2 = (s32[4,32]{1,0:T(4,128)S(1)}, s32[4,32]{1,0:T(4,128)S(1)}, u32[]{:S(2)}, u32[]{:S(2)}) collective-permute-start(s32[4,32]{1,0:T(4,128)S(1)} %reshape.186), channel_id=1, source_target_pairs={{0,4},{4,8},{8,12},{12,16},{16,20},{20,24},{24,28},{1,5},{5,9},{9,... | collective-permute-start | bytes 1544 | tf_op jit(solution)/shard_map/ppermute | solution.py:21
  15.8 6.0 %all_gather.21 = bf16[128,1024]{1,0:T(8,128)(2,1)S(1)} all-gather(bf16[128,256]{1,0:T(8,128)(2,1)} %param.8), channel_id=1, replica_groups=mesh['sp'=8,'tp'=4] {'tp'}, dimensions={1}, use_global_device_ids=true | all-gather | bytes 327680 | tf_op jit(solution)/shard_map/all_gather | solution.py:84
  23.8 3.5 %gather_fusion = f32[1024,4,8]{2,1,0:T(4,128)S(1)} fusion(f32[4,8,16]{1,0,2:T(4,128)S(1)} %bitcast.251, s32[1024]{0:T(1024)S(1)} %broadcast_clamp_fusion), kind=kCustom, calls=%fused_computation | custom fusion | bytes 266240 | tf_op jit(solution)/shard_map/gather | solution.py:55
  29.0 27.4 %all-gather.5.cloned.1.call-done = bf16[3,1024,256]{2,1,0:T(8,128)(2,1)} async-done(((bf16[3,128,256]{2,1,0:T(8,128)(2,1)}), bf16[3,1024,256]{2,1,0:T(8,128)(2,1)}) %all-gather.5.cloned.1.call-update) | async-done | bytes 1572880 | tf_op jit(solution)/shard_map/all_gather | solution.py:78
  56.4 1.3 fusion.17
  58.4 42.8 %all-gather.7.cloned.1.call-done = bf16[3,1024,256]{2,1,0:T(8,128)(2,1)} async-done(((bf16[3,128,256]{2,1,0:T(8,128)(2,1)}), bf16[3,1024,256]{2,1,0:T(8,128)(2,1)}) %all-gather.7.cloned.1.call-update) | async-done | bytes 1572880 | tf_op jit(solution)/shard_map/all_gather | solution.py:79
  101.2 1.3 convolution_convert_fusion.10
  102.8 2.5 collective-permute-start
  106.5 39.4 %all-gather.9.cloned.1.call-done = bf16[3,1024,256]{2,1,0:T(8,128)(2,1)} async-done(((bf16[3,128,256]{2,1,0:T(8,128)(2,1)}), bf16[3,1024,256]{2,1,0:T(8,128)(2,1)}) %all-gather.9.cloned.1.call-update) | async-done | bytes 1572880 | tf_op jit(solution)/shard_map/all_gather | solution.py:77
  146.0 1.3 fusion.16
  150.8 39.8 %all-gather.11.cloned.1.call-done = bf16[3,256,1024]{2,1,0:T(8,128)(2,1)} async-done(((bf16[3,256,128]{2,1,0:T(8,128)(2,1)}), bf16[3,256,1024]{2,1,0:T(8,128)(2,1)}) %all-gather.11.cloned.1.call-update) | async-done | bytes 1572880 | tf_op jit(solution)/shard_map/all_gather | solution.py:80
  190.7 2.0 convolution_convert_fusion.2
  192.8 3.6 %gather_fusion.1 = f32[1024,4,8]{2,1,0:T(4,128)S(1)} fusion(f32[4,8,16]{1,0,2:T(4,128)S(1)} %bitcast.252, s32[1024]{0:T(1024)S(1)} %broadcast_clamp_fusion), kind=kCustom, calls=%fused_computation.1 | custom fusion | bytes 266240 | tf_op jit(solution)/shard_map/gather | solution.py:55
  197.6 13.6 %reduce-scatter.4.cloned.1.call-done = bf16[128,256]{1,0:T(8,128)(2,1)} async-done(((bf16[128,1024]{1,0:T(8,128)(2,1)}), bf16[128,256]{1,0:T(8,128)(2,1)}) %reduce-scatter.4.cloned.1.call-update) | async-done | bytes 65552 | tf_op jit(solution)/shard_map/reduce_scatter | solution.py:106
  211.2 6.0 %all_gather.26 = bf16[128,1024]{1,0:T(8,128)(2,1)S(1)} all-gather(bf16[128,256]{1,0:T(8,128)(2,1)} %reduce-scatter.4.cloned.1.call-done), channel_id=1, replica_groups=mesh['sp'=8,'tp'=4] {'tp'}, dimensions={1}, use_global_device_ids=true | all-gather | bytes 327680 | tf_op jit(solution)/shard_map/all_gather | solution.py:84
  217.4 1.3 fusion.15
  219.3 1.3 convolution_convert_fusion.7
  220.9 3.4 %collective-permute-start.4 = (bf16[4,32,4,128]{3,1,2,0:T(8,128)(2,1)S(1)}, bf16[4,32,4,128]{3,1,2,0:T(8,128)(2,1)S(1)}, u32[]{:S(2)}, u32[]{:S(2)}) collective-permute-start(bf16[4,32,4,128]{3,1,2,0:T(8,128)(2,1)S(1)} %pad_maximum_fusion.4), channel_id=1, source_target_pairs={{0,4},{4,8},{8,12},{12,16},{16,20},{20,24},{24,28},{1,5},{5,9},{9,... | collective-permute-start | bytes 393224 | tf_op jit(solution)/shard_map/ppermute | solution.py:21
  224.3 1.5 collective-permute-start.5
  225.8 1.3 fusion.14
  227.7 3.9 %collective-permute-done.5 = bf16[4,32,4,128]{3,1,2,0:T(8,128)(2,1)S(1)} collective-permute-done((bf16[4,32,4,128]{3,1,2,0:T(8,128)(2,1)S(1)}, bf16[4,32,4,128]{3,1,2,0:T(8,128)(2,1)S(1)}, u32[]{:S(2)}, u32[]{:S(2)}) %collective-permute-start.5) | collective-permute-done | bytes 131104 | tf_op jit(solution)/shard_map/ppermute | solution.py:22
  234.6 2.0 convolution_convert_fusion.1
  236.7 3.5 %gather_fusion.2 = f32[1024,4,8]{2,1,0:T(4,128)S(1)} fusion(f32[4,8,16]{1,0,2:T(4,128)S(1)} %bitcast.250, s32[1024]{0:T(1024)S(1)} %broadcast_clamp_fusion), kind=kCustom, calls=%fused_computation.2 | custom fusion | bytes 266240 | tf_op jit(solution)/shard_map/gather | solution.py:55
  241.5 15.2 %reduce-scatter.6.cloned.1.call-done = bf16[128,256]{1,0:T(8,128)(2,1)} async-done(((bf16[128,1024]{1,0:T(8,128)(2,1)}), bf16[128,256]{1,0:T(8,128)(2,1)}) %reduce-scatter.6.cloned.1.call-update) | async-done | bytes 65552 | tf_op jit(solution)/shard_map/reduce_scatter | solution.py:106
  256.7 6.0 %all_gather.27 = bf16[128,1024]{1,0:T(8,128)(2,1)S(1)} all-gather(bf16[128,256]{1,0:T(8,128)(2,1)} %reduce-scatter.6.cloned.1.call-done), channel_id=1, replica_groups=mesh['sp'=8,'tp'=4] {'tp'}, dimensions={1}, use_global_device_ids=true | all-gather | bytes 327680 | tf_op jit(solution)/shard_map/all_gather | solution.py:84
  262.9 1.3 fusion.13
  264.8 1.3 convolution_convert_fusion.4
  266.4 3.4 %collective-permute-start.6 = (bf16[4,32,4,128]{3,1,2,0:T(8,128)(2,1)S(1)}, bf16[4,32,4,128]{3,1,2,0:T(8,128)(2,1)S(1)}, u32[]{:S(2)}, u32[]{:S(2)}) collective-permute-start(bf16[4,32,4,128]{3,1,2,0:T(8,128)(2,1)S(1)} %pad_maximum_fusion.5), channel_id=1, source_target_pairs={{0,4},{4,8},{8,12},{12,16},{16,20},{20,24},{24,28},{1,5},{5,9},{9,... | collective-permute-start | bytes 393224 | tf_op jit(solution)/shard_map/ppermute | solution.py:21
  271.1 1.3 fusion.12
  273.1 4.1 %collective-permute-done.7 = bf16[4,32,4,128]{3,1,2,0:T(8,128)(2,1)S(1)} collective-permute-done((bf16[4,32,4,128]{3,1,2,0:T(8,128)(2,1)S(1)}, bf16[4,32,4,128]{3,1,2,0:T(8,128)(2,1)S(1)}, u32[]{:S(2)}, u32[]{:S(2)}) %collective-permute-start.7) | collective-permute-done | bytes 131104 | tf_op jit(solution)/shard_map/ppermute | solution.py:22
  280.1 2.0 convolution_convert_fusion
  282.1 20.2 %reduce-scatter.8.cloned.1.call-done = bf16[128,256]{1,0:T(8,128)(2,1)} async-done(((bf16[128,1024]{1,0:T(8,128)(2,1)}), bf16[128,256]{1,0:T(8,128)(2,1)}) %reduce-scatter.8.cloned.1.call-update) | async-done | bytes 65552 | tf_op jit(solution)/shard_map/reduce_scatter | solution.py:106
  (133 shorter events, 26.4 us)
Async XLA Ops:
  6.5 49.9 %all-gather.5.cloned.1.call-start = ((), (), s32[]{:S(2)}) async-start(), calls=%async_computation.3 | async-start | bytes 1769472 | tf_op jit(solution)/shard_map/all_gather | solution.py:78
  7.3 93.9 %all-gather.7.cloned.1.call-start = ((), (), s32[]{:S(2)}) async-start(), calls=%async_computation.4 | async-start | bytes 1769472 | tf_op jit(solution)/shard_map/all_gather | solution.py:79
  8.0 137.9 %all-gather.9.cloned.1.call-start = ((), (), s32[]{:S(2)}) async-start(), calls=%async_computation.5 | async-start | bytes 1769472 | tf_op jit(solution)/shard_map/all_gather | solution.py:77
  8.7 181.9 %all-gather.11.cloned.1.call-start = ((), (), s32[]{:S(2)}) async-start(), calls=%async_computation.6 | async-start | bytes 1769472 | tf_op jit(solution)/shard_map/all_gather | solution.py:80
  9.5 19.1 %collective-permute-start.2 = (s32[4,32]{1,0:T(4,128)S(1)}, s32[4,32]{1,0:T(4,128)S(1)}, u32[]{:S(2)}, u32[]{:S(2)}) collective-permute-start(s32[4,32]{1,0:T(4,128)S(1)} %reshape.186), channel_id=1, source_target_pairs={{0,4},{4,8},{8,12},{12,16},{16,20},{20,24},{24,28},{1,5},{5,9},{9,... | collective-permute-start | bytes 1544 | tf_op jit(solution)/shard_map/ppermute | solution.py:21
  14.4 14.2 %collective-permute-start.3 = (s32[4,32]{1,0:T(4,128)S(1)}, s32[4,32]{1,0:T(4,128)S(1)}, u32[]{:S(2)}, u32[]{:S(2)}) collective-permute-start(s32[4,32]{1,0:T(4,128)S(1)} %reshape.186), channel_id=1, source_target_pairs={{4,0},{8,4},{12,8},{16,12},{20,16},{24,20},{28,24},{5,1},{9,5},{13... | collective-permute-start | bytes 1544 | tf_op jit(solution)/shard_map/ppermute | solution.py:22
  15.7 195.5 %reduce-scatter.4.cloned.1.call-start = ((), (), s32[]{:S(2)}) async-start(), calls=%async_computation.7 | async-start | bytes 327680 | tf_op jit(solution)/shard_map/reduce_scatter | solution.py:106
  102.8 45.1 %collective-permute-start = (bf16[4,32,4,128]{3,1,2,0:T(8,128)(2,1)S(1)}, bf16[4,32,4,128]{3,1,2,0:T(8,128)(2,1)S(1)}, u32[]{:S(2)}, u32[]{:S(2)}) collective-permute-start(bf16[4,32,4,128]{3,1,2,0:T(8,128)(2,1)S(1)} %pad_maximum_fusion.3), channel_id=1, source_target_pairs={{0,4},{4,8},{8,12},{12,16},{16,20},{20,24},{24,28},{1,5},{5,9},{9,... | collective-permute-start | bytes 393224 | tf_op jit(solution)/shard_map/ppermute | solution.py:21
  105.2 42.7 %collective-permute-start.1 = (bf16[4,32,4,128]{3,1,2,0:T(8,128)(2,1)S(1)}, bf16[4,32,4,128]{3,1,2,0:T(8,128)(2,1)S(1)}, u32[]{:S(2)}, u32[]{:S(2)}) collective-permute-start(bf16[4,32,4,128]{3,1,2,0:T(8,128)(2,1)S(1)} %pad_maximum_fusion.3), channel_id=1, source_target_pairs={{4,0},{8,4},{12,8},{16,12},{20,16},{24,20},{28,24},{5,1},{9,5},{13... | collective-permute-start | bytes 393224 | tf_op jit(solution)/shard_map/ppermute | solution.py:22
  192.7 64.1 %reduce-scatter.6.cloned.1.call-start = ((), (), s32[]{:S(2)}) async-start(), calls=%async_computation.8 | async-start | bytes 327680 | tf_op jit(solution)/shard_map/reduce_scatter | solution.py:106
  220.9 6.8 %collective-permute-start.4 = (bf16[4,32,4,128]{3,1,2,0:T(8,128)(2,1)S(1)}, bf16[4,32,4,128]{3,1,2,0:T(8,128)(2,1)S(1)}, u32[]{:S(2)}, u32[]{:S(2)}) collective-permute-start(bf16[4,32,4,128]{3,1,2,0:T(8,128)(2,1)S(1)} %pad_maximum_fusion.4), channel_id=1, source_target_pairs={{0,4},{4,8},{8,12},{12,16},{16,20},{20,24},{24,28},{1,5},{5,9},{9,... | collective-permute-start | bytes 393224 | tf_op jit(solution)/shard_map/ppermute | solution.py:21
  224.3 7.4 %collective-permute-start.5 = (bf16[4,32,4,128]{3,1,2,0:T(8,128)(2,1)S(1)}, bf16[4,32,4,128]{3,1,2,0:T(8,128)(2,1)S(1)}, u32[]{:S(2)}, u32[]{:S(2)}) collective-permute-start(bf16[4,32,4,128]{3,1,2,0:T(8,128)(2,1)S(1)} %pad_maximum_fusion.4), channel_id=1, source_target_pairs={{4,0},{8,4},{12,8},{16,12},{20,16},{24,20},{28,24},{5,1},{9,5},{13... | collective-permute-start | bytes 393224 | tf_op jit(solution)/shard_map/ppermute | solution.py:22
  236.6 65.7 %reduce-scatter.8.cloned.1.call-start = ((), (), s32[]{:S(2)}) async-start(), calls=%async_computation.9 | async-start | bytes 327680 | tf_op jit(solution)/shard_map/reduce_scatter | solution.py:106
  266.4 6.6 %collective-permute-start.6 = (bf16[4,32,4,128]{3,1,2,0:T(8,128)(2,1)S(1)}, bf16[4,32,4,128]{3,1,2,0:T(8,128)(2,1)S(1)}, u32[]{:S(2)}, u32[]{:S(2)}) collective-permute-start(bf16[4,32,4,128]{3,1,2,0:T(8,128)(2,1)S(1)} %pad_maximum_fusion.5), channel_id=1, source_target_pairs={{0,4},{4,8},{8,12},{12,16},{16,20},{20,24},{24,28},{1,5},{5,9},{9,... | collective-permute-start | bytes 393224 | tf_op jit(solution)/shard_map/ppermute | solution.py:21
  269.8 7.4 %collective-permute-start.7 = (bf16[4,32,4,128]{3,1,2,0:T(8,128)(2,1)S(1)}, bf16[4,32,4,128]{3,1,2,0:T(8,128)(2,1)S(1)}, u32[]{:S(2)}, u32[]{:S(2)}) collective-permute-start(bf16[4,32,4,128]{3,1,2,0:T(8,128)(2,1)S(1)} %pad_maximum_fusion.5), channel_id=1, source_target_pairs={{4,0},{8,4},{12,8},{16,12},{20,16},{24,20},{28,24},{5,1},{9,5},{13... | collective-permute-start | bytes 393224 | tf_op jit(solution)/shard_map/ppermute | solution.py:22
Sparse Core Ops, SparseCore 0:
  9.5 46.8 all-gather.4
  58.6 42.5 all-gather.6
  103.4 42.5 all-gather.8
  147.8 42.7 all-gather.10
  193.0 18.2 reduce-scatter.3
  236.7 19.9 reduce-scatter.5
  282.2 20.0 reduce-scatter.7
where the time goes:
time: 310 us; the launch traced here: 309 us
  waiting for transfers between devices  209 us (67%)
  matrix products  23 us (7%)
  starting transfers between devices  19.7 us (6%)
  local copies, waits for them, and re-layouts  19.3 us (6%)
  blocking collectives  17.9 us (6%)
  between operations  14.2 us (5%)
  other arithmetic  6.3 us (2%)
    reduce_scatter x3, waiting for transfers between devices, body(): lax.psum_scatter(partial_sums.astype(jnp.bfloat16), 'tp', scatter_dimensi...  49 us
    all_gather x1, waiting for transfers between devices, body(): lax.all_gather(w_value, 'sp', axis=1, tiled=True)  42.8 us
    all_gather x1, waiting for transfers between devices, body(): lax.all_gather(w_out, 'sp', axis=2, tiled=True)  39.8 us
    all_gather x1, waiting for transfers between devices, body(): lax.all_gather(w_query, 'sp', axis=1, tiled=True)  39.4 us
    all_gather x1, waiting for transfers between devices, body(): lax.all_gather(w_key, 'sp', axis=1, tiled=True)  27.4 us
    all_gather x3, blocking collectives, body(): gathered = lax.all_gather(stream, 'tp', axis=1, tiled=True)  17.9 us
    gather x6, local copies, waits for them, and re-layouts, attend(): bias_table = bias_layer[:, :, jnp.clip(col_offset, 0, WIN_COLS - 1)]  14.4 us
    ppermute x4, starting transfers between devices, with_halo(): before = lax.ppermute(last, axis, up)  14.1 us
  transfers between devices with their start and end apart: 15, of which 9 were waited for; matrix products, arithmetic and copies ran while one was open for 10% of the time, Pallas kernels for 0%

commit v1 on v0

--- a/solution.py
+++ b/solution.py
@@ -9,6 +9,33 @@
 LAYERS = 3
 GRID_W = 32
 EPS = 1e-06
+
+
+def _end_chains(local_block, axis_no):
+    lower = list(local_block.shape[1:])
+    lower[axis_no] *= local_block.shape[0]
+    n_now = jnp.moveaxis(local_block, 0, axis_no).reshape(lower)
+    return n_now
+
+
+def tails_cut(local_values, named_axis):
+    now, back = (lax.axis_size(named_axis), lax.axis_index(named_axis))
+    block_now, outcome_arr = (local_values[None], 1)
+    while outcome_arr < now:
+        piece_now = lax.ppermute(
+            block_now, axis_name=named_axis, perm=[(idx, idx ^ outcome_arr) for idx in range(now)]
+        )
+        all_rows = back & outcome_arr == 0
+        block_now = jnp.concatenate(
+            [jnp.where(all_rows, block_now, piece_now), jnp.where(all_rows, piece_now, block_now)]
+        )
+        outcome_arr *= 2
+    return block_now
+
+
+def apply_the_lane(which_dim, w_in, shard_in):
+    res = _end_chains(tails_cut(w_in, shard_in), which_dim)
+    return res
 
 
 def with_halo(shard, sides, width, wrap):
@@ -81,7 +108,7 @@
     )
     stream = tokens
     for layer_index in range(LAYERS):
-        gathered = lax.all_gather(stream, "tp", axis=1, tiled=True)
+        gathered = apply_the_lane(1, stream, "tp")
         normed = rms_rows(gathered, norm_gain[layer_index])
         query_raw = jnp.dot(normed, collected[0][layer_index], preferred_element_type=jnp.float32)
         key_raw = jnp.dot(normed, collected[1][layer_index], preferred_element_type=jnp.float32)

time: 310 us -> 316 us (1.019)
  waiting for transfers between devices: 209 us -> 227 us
  blocking collectives: 17.9 us -> 0 us
    all_gather x3 -> x0, blocking collectives: 17.9 us -> none  [body(): gathered = lax.all_gather(stream, 'tp', axis=1, tiled=True)]
    reduce_scatter x3, waiting for transfers between devices: 49 us -> 60.6 us  [body(): lax.psum_scatter(partial_sums.astype(jnp.bfloat16), 'tp', scatter_dimensi...]
    ppermute x0 -> x6, waiting for transfers between devices: none -> 7.84 us  [tails_cut(): lax.ppermute(block_now, axis_name=named_axis, perm=[(idx, idx ^ outcome_a...]
  transfers between devices with their start and end apart: 15 -> 21, of which waited for: 9 -> 14; matrix products, arithmetic and copies ran while one was open for 10% -> 10% of each run, Pallas kernels for 0% -> 0%
where the time goes in v1:
time: 316 us; the launch traced here: 315 us
  waiting for transfers between devices  227 us (72%)
  matrix products  22.9 us (7%)
  starting transfers between devices  22 us (7%)
  local copies, waits for them, and re-layouts  19.9 us (6%)
  between operations  14.3 us (5%)
  other arithmetic  8.58 us (3%)
    reduce_scatter x3, waiting for transfers between devices, body(): lax.psum_scatter(partial_sums.astype(jnp.bfloat16), 'tp', scatter_dimensi...  60.6 us
    all_gather x1, waiting for transfers between devices, body(): lax.all_gather(w_value, 'sp', axis=1, tiled=True)  42.8 us
    all_gather x1, waiting for transfers between devices, body(): lax.all_gather(w_out, 'sp', axis=2, tiled=True)  39.8 us
    all_gather x1, waiting for transfers between devices, body(): lax.all_gather(w_query, 'sp', axis=1, tiled=True)  39.4 us
    all_gather x1, waiting for transfers between devices, body(): lax.all_gather(w_key, 'sp', axis=1, tiled=True)  27.2 us
    gather x6, local copies, waits for them, and re-layouts, attend(): bias_table = bias_layer[:, :, jnp.clip(col_offset, 0, WIN_COLS - 1)]  14.4 us
    ppermute x4, starting transfers between devices, with_halo(): before = lax.ppermute(last, axis, up)  14.1 us
    ppermute x6, waiting for transfers between devices, tails_cut(): lax.ppermute(block_now, axis_name=named_axis, perm=[(idx, idx ^ outcome_a...  7.84 us
  transfers between devices with their start and end apart: 21, of which 14 were waited for; matrix products, arithmetic and copies ran while one was open for 10% of the time, Pallas kernels for 0%

profile of v1, /device:TPU:0, one launch (start us, length us, event | category | flops | bytes accessed | tf_op | source)
XLA Modules:
  0.0 314.6 jit_solution(18083222385793629556)
XLA Ops:
  9.5 4.9 %collective-permute-start.4 = (s32[4,32]{1,0:T(4,128)S(1)}, s32[4,32]{1,0:T(4,128)S(1)}, u32[]{:S(2)}, u32[]{:S(2)}) collective-permute-start(s32[4,32]{1,0:T(4,128)S(1)} %reshape.288), channel_id=1, source_target_pairs={{0,4},{4,8},{8,12},{12,16},{16,20},{20,24},{24,28},{1,5},{5,9},{9,... | collective-permute-start | bytes 1544 | tf_op jit(solution)/shard_map/ppermute | solution.py:48
  17.8 3.6 %gather_fusion = f32[1024,4,8]{2,1,0:T(4,128)S(1)} fusion(f32[4,8,16]{1,0,2:T(4,128)S(1)} %bitcast.275, s32[1024]{0:T(1024)S(1)} %broadcast_clamp_fusion), kind=kCustom, calls=%fused_computation | custom fusion | bytes 266240 | tf_op jit(solution)/shard_map/gather | solution.py:82
  22.8 1.6 collective-permute-start.1
  24.6 4.2 %collective-permute-done.1 = bf16[2,128,256]{2,1,0:T(8,128)(2,1)S(1)} collective-permute-done((bf16[2,128,256]{2,1,0:T(8,128)(2,1)S(1)}, bf16[2,128,256]{2,1,0:T(8,128)(2,1)S(1)}, u32[]{:S(2)}, u32[]{:S(2)}) %collective-permute-start.1) | collective-permute-done | bytes 131104 | tf_op jit(solution)/shard_map/ppermute | solution.py:25
  29.3 27.2 %all-gather.5.cloned.1.call-done = bf16[3,1024,256]{2,1,0:T(8,128)(2,1)} async-done(((bf16[3,128,256]{2,1,0:T(8,128)(2,1)}), bf16[3,1024,256]{2,1,0:T(8,128)(2,1)}) %all-gather.5.cloned.1.call-update) | async-done | bytes 1572880 | tf_op jit(solution)/shard_map/all_gather | solution.py:105
  58.4 42.8 %all-gather.7.cloned.1.call-done = bf16[3,1024,256]{2,1,0:T(8,128)(2,1)} async-done(((bf16[3,128,256]{2,1,0:T(8,128)(2,1)}), bf16[3,1024,256]{2,1,0:T(8,128)(2,1)}) %all-gather.7.cloned.1.call-update) | async-done | bytes 1572880 | tf_op jit(solution)/shard_map/all_gather | solution.py:106
  101.3 1.3 convolution_convert_fusion.10
  102.8 2.5 collective-permute-start.2
  106.6 39.4 %all-gather.9.cloned.1.call-done = bf16[3,1024,256]{2,1,0:T(8,128)(2,1)} async-done(((bf16[3,128,256]{2,1,0:T(8,128)(2,1)}), bf16[3,1024,256]{2,1,0:T(8,128)(2,1)}) %all-gather.9.cloned.1.call-update) | async-done | bytes 1572880 | tf_op jit(solution)/shard_map/all_gather | solution.py:104
  146.0 1.3 fusion.16
  150.9 39.8 %all-gather.11.cloned.1.call-done = bf16[3,256,1024]{2,1,0:T(8,128)(2,1)} async-done(((bf16[3,256,128]{2,1,0:T(8,128)(2,1)}), bf16[3,256,1024]{2,1,0:T(8,128)(2,1)}) %all-gather.11.cloned.1.call-update) | async-done | bytes 1572880 | tf_op jit(solution)/shard_map/all_gather | solution.py:107
  190.7 2.0 convolution_convert_fusion.2
  192.8 18.5 %reduce-scatter.4.cloned.1.call-done = bf16[128,256]{1,0:T(8,128)(2,1)} async-done(((bf16[128,1024]{1,0:T(8,128)(2,1)}), bf16[128,256]{1,0:T(8,128)(2,1)}) %reduce-scatter.4.cloned.1.call-update) | async-done | bytes 65552 | tf_op jit(solution)/shard_map/reduce_scatter | solution.py:133
  211.3 1.5 collective-permute-done.6
  214.1 3.6 %gather_fusion.1 = f32[1024,4,8]{2,1,0:T(4,128)S(1)} fusion(f32[4,8,16]{1,0,2:T(4,128)S(1)} %bitcast.276, s32[1024]{0:T(1024)S(1)} %broadcast_clamp_fusion), kind=kCustom, calls=%fused_computation.1 | custom fusion | bytes 266240 | tf_op jit(solution)/shard_map/gather | solution.py:82
  219.8 1.3 fusion.15
  221.7 1.3 convolution_convert_fusion.7
  223.3 3.4 %collective-permute-start.8 = (bf16[4,32,4,128]{3,1,2,0:T(8,128)(2,1)S(1)}, bf16[4,32,4,128]{3,1,2,0:T(8,128)(2,1)S(1)}, u32[]{:S(2)}, u32[]{:S(2)}) collective-permute-start(bf16[4,32,4,128]{3,1,2,0:T(8,128)(2,1)S(1)} %pad_maximum_fusion.9), channel_id=1, source_target_pairs={{0,4},{4,8},{8,12},{12,16},{16,20},{20,24},{24,28},{1,5},{5,9},{9,... | collective-permute-start | bytes 393224 | tf_op jit(solution)/shard_map/ppermute | solution.py:48
  226.7 1.5 collective-permute-start.9
  228.2 1.3 fusion.14
  230.1 3.4 %collective-permute-done.9 = bf16[4,32,4,128]{3,1,2,0:T(8,128)(2,1)S(1)} collective-permute-done((bf16[4,32,4,128]{3,1,2,0:T(8,128)(2,1)S(1)}, bf16[4,32,4,128]{3,1,2,0:T(8,128)(2,1)S(1)}, u32[]{:S(2)}, u32[]{:S(2)}) %collective-permute-start.9) | collective-permute-done | bytes 131104 | tf_op jit(solution)/shard_map/ppermute | solution.py:49
  236.5 2.0 convolution_convert_fusion.1
  238.5 21.0 %reduce-scatter.6.cloned.1.call-done = bf16[128,256]{1,0:T(8,128)(2,1)} async-done(((bf16[128,1024]{1,0:T(8,128)(2,1)}), bf16[128,256]{1,0:T(8,128)(2,1)}) %reduce-scatter.6.cloned.1.call-update) | async-done | bytes 65552 | tf_op jit(solution)/shard_map/reduce_scatter | solution.py:133
  259.5 1.5 collective-permute-done.10
  262.3 3.6 %gather_fusion.2 = f32[1024,4,8]{2,1,0:T(4,128)S(1)} fusion(f32[4,8,16]{1,0,2:T(4,128)S(1)} %bitcast.274, s32[1024]{0:T(1024)S(1)} %broadcast_clamp_fusion), kind=kCustom, calls=%fused_computation.2 | custom fusion | bytes 266240 | tf_op jit(solution)/shard_map/gather | solution.py:82
  268.0 1.3 fusion.13
  269.9 1.3 convolution_convert_fusion.4
  271.5 3.4 %collective-permute-start.12 = (bf16[4,32,4,128]{3,1,2,0:T(8,128)(2,1)S(1)}, bf16[4,32,4,128]{3,1,2,0:T(8,128)(2,1)S(1)}, u32[]{:S(2)}, u32[]{:S(2)}) collective-permute-start(bf16[4,32,4,128]{3,1,2,0:T(8,128)(2,1)S(1)} %pad_maximum_fusion.11), channel_id=1, source_target_pairs={{0,4},{4,8},{8,12},{12,16},{16,20},{20,24},{24,28},{1,5},{5,9},{9,... | collective-permute-start | bytes 393224 | tf_op jit(solution)/shard_map/ppermute | solution.py:48
  276.2 1.3 fusion.12
  278.2 3.6 %collective-permute-done.13 = bf16[4,32,4,128]{3,1,2,0:T(8,128)(2,1)S(1)} collective-permute-done((bf16[4,32,4,128]{3,1,2,0:T(8,128)(2,1)S(1)}, bf16[4,32,4,128]{3,1,2,0:T(8,128)(2,1)S(1)}, u32[]{:S(2)}, u32[]{:S(2)}) %collective-permute-start.13) | collective-permute-done | bytes 131104 | tf_op jit(solution)/shard_map/ppermute | solution.py:49
  284.7 2.0 convolution_convert_fusion
  286.7 21.0 %reduce-scatter.8.cloned.1.call-done = bf16[128,256]{1,0:T(8,128)(2,1)} async-done(((bf16[128,1024]{1,0:T(8,128)(2,1)}), bf16[128,256]{1,0:T(8,128)(2,1)}) %reduce-scatter.8.cloned.1.call-update) | async-done | bytes 65552 | tf_op jit(solution)/shard_map/reduce_scatter | solution.py:133
  (162 shorter events, 32.0 us)
Async XLA Ops:
  6.5 50.0 %all-gather.5.cloned.1.call-start = ((), (), s32[]{:S(2)}) async-start(), calls=%async_computation.3 | async-start | bytes 1769472 | tf_op jit(solution)/shard_map/all_gather | solution.py:105
  7.3 94.0 %all-gather.7.cloned.1.call-start = ((), (), s32[]{:S(2)}) async-start(), calls=%async_computation.4 | async-start | bytes 1769472 | tf_op jit(solution)/shard_map/all_gather | solution.py:106
  8.0 138.0 %all-gather.9.cloned.1.call-start = ((), (), s32[]{:S(2)}) async-start(), calls=%async_computation.5 | async-start | bytes 1769472 | tf_op jit(solution)/shard_map/all_gather | solution.py:104
  8.7 182.0 %all-gather.11.cloned.1.call-start = ((), (), s32[]{:S(2)}) async-start(), calls=%async_computation.6 | async-start | bytes 1769472 | tf_op jit(solution)/shard_map/all_gather | solution.py:107
  9.5 13.1 %collective-permute-start.4 = (s32[4,32]{1,0:T(4,128)S(1)}, s32[4,32]{1,0:T(4,128)S(1)}, u32[]{:S(2)}, u32[]{:S(2)}) collective-permute-start(s32[4,32]{1,0:T(4,128)S(1)} %reshape.288), channel_id=1, source_target_pairs={{0,4},{4,8},{8,12},{12,16},{16,20},{20,24},{24,28},{1,5},{5,9},{9,... | collective-permute-start | bytes 1544 | tf_op jit(solution)/shard_map/ppermute | solution.py:48
  14.4 8.2 %collective-permute-start.5 = (s32[4,32]{1,0:T(4,128)S(1)}, s32[4,32]{1,0:T(4,128)S(1)}, u32[]{:S(2)}, u32[]{:S(2)}) collective-permute-start(s32[4,32]{1,0:T(4,128)S(1)} %reshape.288), channel_id=1, source_target_pairs={{4,0},{8,4},{12,8},{16,12},{20,16},{24,20},{28,24},{5,1},{9,5},{13... | collective-permute-start | bytes 1544 | tf_op jit(solution)/shard_map/ppermute | solution.py:49
  15.7 7.1 %copy-start = (bf16[128,256]{1,0:T(8,128)(2,1)S(1)}, bf16[128,256]{1,0:T(8,128)(2,1)}, u32[]{:S(2)}) copy-start(bf16[128,256]{1,0:T(8,128)(2,1)} %param.8) | copy-start | bytes 196612
  15.7 7.0 %collective-permute-start = (bf16[1,128,256]{2,1,0:T(8,128)(2,1)}, bf16[1,128,256]{2,1,0:T(8,128)(2,1)S(1)}, u32[]{:S(2)}, u32[]{:S(2)}) collective-permute-start(bf16[1,128,256]{2,1,0:T(8,128)(2,1)} %bitcast.301), channel_id=1, source_target_pairs={{0,1},{1,0},{2,3},{3,2},{4,5},{5,4},{6,7},{7,6},{8,9},{9,8},{10,11... | collective-permute-start | bytes 196616 | tf_op jit(solution)/shard_map/ppermute | solution.py:25
  15.8 195.5 %reduce-scatter.4.cloned.1.call-start = ((), (), s32[]{:S(2)}) async-start(), calls=%async_computation.7 | async-start | bytes 327680 | tf_op jit(solution)/shard_map/reduce_scatter | solution.py:133
  22.8 6.0 %collective-permute-start.1 = (bf16[2,128,256]{2,1,0:T(8,128)(2,1)S(1)}, bf16[2,128,256]{2,1,0:T(8,128)(2,1)S(1)}, u32[]{:S(2)}, u32[]{:S(2)}) collective-permute-start(bf16[2,128,256]{2,1,0:T(8,128)(2,1)S(1)} %pad_maximum_fusion.6), channel_id=1, source_target_pairs={{0,2},{1,3},{2,0},{3,1},{4,6},{5,7},{6,4},{7,5},{8,10},{9,11},{10,... | collective-permute-start | bytes 393224 | tf_op jit(solution)/shard_map/ppermute | solution.py:25
  102.8 45.1 %collective-permute-start.2 = (bf16[4,32,4,128]{3,1,2,0:T(8,128)(2,1)S(1)}, bf16[4,32,4,128]{3,1,2,0:T(8,128)(2,1)S(1)}, u32[]{:S(2)}, u32[]{:S(2)}) collective-permute-start(bf16[4,32,4,128]{3,1,2,0:T(8,128)(2,1)S(1)} %pad_maximum_fusion.7), channel_id=1, source_target_pairs={{0,4},{4,8},{8,12},{12,16},{16,20},{20,24},{24,28},{1,5},{5,9},{9,... | collective-permute-start | bytes 393224 | tf_op jit(solution)/shard_map/ppermute | solution.py:48
  105.3 42.7 %collective-permute-start.3 = (bf16[4,32,4,128]{3,1,2,0:T(8,128)(2,1)S(1)}, bf16[4,32,4,128]{3,1,2,0:T(8,128)(2,1)S(1)}, u32[]{:S(2)}, u32[]{:S(2)}) collective-permute-start(bf16[4,32,4,128]{3,1,2,0:T(8,128)(2,1)S(1)} %pad_maximum_fusion.7), channel_id=1, source_target_pairs={{4,0},{8,4},{12,8},{16,12},{20,16},{24,20},{28,24},{5,1},{9,5},{13... | collective-permute-start | bytes 393224 | tf_op jit(solution)/shard_map/ppermute | solution.py:49
  192.8 66.8 %reduce-scatter.6.cloned.1.call-start = ((), (), s32[]{:S(2)}) async-start(), calls=%async_computation.8 | async-start | bytes 327680 | tf_op jit(solution)/shard_map/reduce_scatter | solution.py:133
  211.3 1.5 collective-permute-start.6
  213.7 5.6 %collective-permute-start.7 = (bf16[2,128,256]{2,1,0:T(8,128)(2,1)S(1)}, bf16[2,128,256]{2,1,0:T(8,128)(2,1)S(1)}, u32[]{:S(2)}, u32[]{:S(2)}) collective-permute-start(bf16[2,128,256]{2,1,0:T(8,128)(2,1)S(1)} %pad_maximum_fusion.8), channel_id=1, source_target_pairs={{0,2},{1,3},{2,0},{3,1},{4,6},{5,7},{6,4},{7,5},{8,10},{9,11},{10,... | collective-permute-start | bytes 393224 | tf_op jit(solution)/shard_map/ppermute | solution.py:25
  223.3 6.8 %collective-permute-start.8 = (bf16[4,32,4,128]{3,1,2,0:T(8,128)(2,1)S(1)}, bf16[4,32,4,128]{3,1,2,0:T(8,128)(2,1)S(1)}, u32[]{:S(2)}, u32[]{:S(2)}) collective-permute-start(bf16[4,32,4,128]{3,1,2,0:T(8,128)(2,1)S(1)} %pad_maximum_fusion.9), channel_id=1, source_target_pairs={{0,4},{4,8},{8,12},{12,16},{16,20},{20,24},{24,28},{1,5},{5,9},{9,... | collective-permute-start | bytes 393224 | tf_op jit(solution)/shard_map/ppermute | solution.py:48
  226.7 6.9 %collective-permute-start.9 = (bf16[4,32,4,128]{3,1,2,0:T(8,128)(2,1)S(1)}, bf16[4,32,4,128]{3,1,2,0:T(8,128)(2,1)S(1)}, u32[]{:S(2)}, u32[]{:S(2)}) collective-permute-start(bf16[4,32,4,128]{3,1,2,0:T(8,128)(2,1)S(1)} %pad_maximum_fusion.9), channel_id=1, source_target_pairs={{4,0},{8,4},{12,8},{16,12},{20,16},{24,20},{28,24},{5,1},{9,5},{13... | collective-permute-start | bytes 393224 | tf_op jit(solution)/shard_map/ppermute | solution.py:49
  238.5 69.3 %reduce-scatter.8.cloned.1.call-start = ((), (), s32[]{:S(2)}) async-start(), calls=%async_computation.9 | async-start | bytes 327680 | tf_op jit(solution)/shard_map/reduce_scatter | solution.py:133
  259.5 1.5 collective-permute-start.10
  261.9 5.6 %collective-permute-start.11 = (bf16[2,128,256]{2,1,0:T(8,128)(2,1)S(1)}, bf16[2,128,256]{2,1,0:T(8,128)(2,1)S(1)}, u32[]{:S(2)}, u32[]{:S(2)}) collective-permute-start(bf16[2,128,256]{2,1,0:T(8,128)(2,1)S(1)} %pad_maximum_fusion.10), channel_id=1, source_target_pairs={{0,2},{1,3},{2,0},{3,1},{4,6},{5,7},{6,4},{7,5},{8,10},{9,11},{10,... | collective-permute-start | bytes 393224 | tf_op jit(solution)/shard_map/ppermute | solution.py:25
  271.5 6.6 %collective-permute-start.12 = (bf16[4,32,4,128]{3,1,2,0:T(8,128)(2,1)S(1)}, bf16[4,32,4,128]{3,1,2,0:T(8,128)(2,1)S(1)}, u32[]{:S(2)}, u32[]{:S(2)}) collective-permute-start(bf16[4,32,4,128]{3,1,2,0:T(8,128)(2,1)S(1)} %pad_maximum_fusion.11), channel_id=1, source_target_pairs={{0,4},{4,8},{8,12},{12,16},{16,20},{20,24},{24,28},{1,5},{5,9},{9,... | collective-permute-start | bytes 393224 | tf_op jit(solution)/shard_map/ppermute | solution.py:48
  274.9 6.9 %collective-permute-start.13 = (bf16[4,32,4,128]{3,1,2,0:T(8,128)(2,1)S(1)}, bf16[4,32,4,128]{3,1,2,0:T(8,128)(2,1)S(1)}, u32[]{:S(2)}, u32[]{:S(2)}) collective-permute-start(bf16[4,32,4,128]{3,1,2,0:T(8,128)(2,1)S(1)} %pad_maximum_fusion.11), channel_id=1, source_target_pairs={{4,0},{8,4},{12,8},{16,12},{20,16},{24,20},{28,24},{5,1},{9,5},{13... | collective-permute-start | bytes 393224 | tf_op jit(solution)/shard_map/ppermute | solution.py:49
Sparse Core Ops, SparseCore 0:
  9.5 46.9 all-gather.4
  58.7 42.5 all-gather.6
  103.4 42.5 all-gather.8
  147.9 42.7 all-gather.10
  193.0 18.2 reduce-scatter.3
  238.6 20.8 reduce-scatter.5
  286.8 20.8 reduce-scatter.7
